TPU v7x, 32 devices: a whole 2x2x4 slice. The times are simulated.
32 devices in a mesh: ep: 8 (over z, core), tp: 4 (over y, x).
Axes of the slice: x: 2, y: 2, z: 4, core: 2. Of those that a mesh axis runs over, the one named last changes fastest.
Arguments:
- queries: bfloat16 [1024, 1536], P('ep', 'tp'), may hold values from -64 to 64
- kv_latent: bfloat16 [1024, 512], P('ep'), may hold values from -60 to 60
- rope_key: bfloat16 [1024, 32], P('ep'), may hold values from -64 to 64
- latent_gain: float32 [512], replicated, may hold values from 0.1 to 1.9
- key_up: bfloat16 [512, 1024], P(None, 'tp'), may hold values from -0.25 to 0.25
- value_up: bfloat16 [512, 1024], P(None, 'tp'), may hold values from -40 to 40
- query_gain: float32 [96], replicated, may hold values from 0.3 to 4
- key_gain: float32 [96], replicated, may hold values from 0.3 to 4
- out_gain: float32 [1024], replicated, may hold values from 0.1 to 1.9
- out_proj: bfloat16 [1024, 4096], P(None, 'tp'), may hold values from -0.1875 to 0.1875
- moe_input: bfloat16 [1024, 4096], P('ep'), may hold values from -60 to 60
- moe_gain: float32 [4096], replicated, may hold values from 0.1 to 1.9
- expert_ids: int32 [1024, 2], P('ep'), may hold values from 0 to 31, as said below
- route_weights: float32 [1024, 2], P('ep'), may hold values from 0.2 to 1
- w_gate: bfloat16 [32, 4096, 2048], P('ep', None, 'tp'), may hold values from -0.09375 to 0.09375
- w_up: bfloat16 [32, 4096, 2048], P('ep', None, 'tp'), may hold values from -0.09375 to 0.09375
- w_down: bfloat16 [32, 2048, 4096], P('ep', 'tp'), may hold values from -0.125 to 0.125
Outputs:
- mixed: bfloat16 [1024, 4096], P('ep', 'tp')
- expert_out: bfloat16 [1024, 4096], P('ep', 'tp')
Inputs may be any that keep to these rules, and one draw needn't show every extreme that they name: `expert_ids`: both experts of a row lie in one group (g * 8 to g * 8 + 7) and differ. In each aligned block of 128 rows no expert is named more than 12 times, and some expert is named exactly 12 times.
All inputs are finite; a program needn't handle non-finite values.
Results may differ from a plain program's by a relative error of at most 0.015.
The roundings to bfloat16 on the way count: a program that leaves them out, or rounds other values in their place, can miss the bound.
Values may be sent and summed in bfloat16 or wider, within the bound.
A program may use at most 128 MiB of HBM per device.

v0:
```python
import jax
import jax.numpy as jnp
from jax import lax
from jax.sharding import PartitionSpec as P

NOPE = 64
ROPE = 32
VDIM = 64
QKD = 96
CAP = 12


EPS = 1e-06
THETA = 10000.0


def rotate_half(values_in, positions):
    half_width = ROPE // 2
    inverse = THETA ** (-jnp.arange(half_width, dtype=jnp.float32) / half_width)
    angles = positions.astype(jnp.float32)[:, None] * inverse
    cosine = jnp.cos(angles)[:, None, :]
    sine = jnp.sin(angles)[:, None, :]
    first_half = values_in[..., :half_width]
    second_half = values_in[..., half_width:]
    return jnp.concatenate(
        [first_half * cosine - second_half * sine, second_half * cosine + first_half * sine],
        axis=-1,
    )


def head_norm(values_in, gain_vec):
    return (
        values_in
        * lax.rsqrt(jnp.mean(values_in * values_in, axis=-1, keepdims=True) + EPS)
        * gain_vec
    )


def make_queries(queries, query_gain, positions):
    row_count = queries.shape[0]
    head_count = queries.shape[1] // QKD
    normed = head_norm(queries.astype(jnp.float32).reshape(row_count, head_count, QKD), query_gain)
    turned = jnp.concatenate(
        [normed[..., :NOPE], rotate_half(normed[..., NOPE:], positions)], axis=-1
    )
    return turned.astype(jnp.bfloat16)


def make_keys(latent, rope_part, latent_gain, key_up, value_up, key_gain, positions):
    row_count = latent.shape[0]
    head_count = key_up.shape[1] // NOPE
    latent_f = latent.astype(jnp.float32)
    latent_n = (
        latent_f
        * lax.rsqrt(jnp.mean(latent_f * latent_f, axis=-1, keepdims=True) + EPS)
        * latent_gain
    ).astype(jnp.bfloat16)
    key_nope = jnp.dot(latent_n, key_up, preferred_element_type=jnp.float32).astype(jnp.bfloat16)
    key_nope = lax.optimization_barrier(key_nope)
    value_rows = jnp.dot(latent_n, value_up, preferred_element_type=jnp.float32).astype(
        jnp.bfloat16
    )
    shared = jnp.broadcast_to(
        rope_part.astype(jnp.float32)[:, None, :], (row_count, head_count, ROPE)
    )
    key_full = jnp.concatenate(
        [key_nope.astype(jnp.float32).reshape(row_count, head_count, NOPE), shared], axis=-1
    )
    normed = head_norm(key_full, key_gain)
    turned = jnp.concatenate(
        [normed[..., :NOPE], rotate_half(normed[..., NOPE:], positions)], axis=-1
    )
    return (turned.astype(jnp.bfloat16), value_rows.reshape(row_count, head_count, VDIM))


def shards(
    queries,
    kv_latent,
    rope_key,
    latent_gain,
    key_up,
    value_up,
    query_gain,
    key_gain,
    out_gain,
    out_proj,
    moe_input,
    moe_gain,
    expert_ids,
    route_weights,
    w_gate,
    w_up,
    w_down,
):
    tok_rows = queries.shape[0]
    head_count = key_up.shape[1] // NOPE
    query_pos = lax.axis_index("ep") * tok_rows + jnp.arange(tok_rows, dtype=jnp.int32)
    query_rot = make_queries(queries, query_gain, query_pos)
    inv_scale = QKD ** (-0.5)
    blocks_in = (
        lax.all_gather(kv_latent, "ep", axis=0, tiled=True),
        lax.all_gather(rope_key, "ep", axis=0, tiled=True),
    )
    key_pos = jnp.arange(blocks_in[0].shape[0], dtype=jnp.int32)
    key_rot, value_rows = make_keys(
        blocks_in[0], blocks_in[1], latent_gain, key_up, value_up, key_gain, key_pos
    )
    top_prev = jnp.full((head_count, tok_rows), -1e30, jnp.float32)
    key_pos = jnp.arange(key_rot.shape[0], dtype=jnp.int32)
    scores = (
        jnp.einsum("qhd,khd->hqk", query_rot, key_rot, preferred_element_type=jnp.float32)
        * inv_scale
    )
    visible = key_pos[None, :] <= query_pos[:, None]
    scores = jnp.where(visible[None], scores, -1e30)
    top_new = jnp.maximum(top_prev, jnp.max(scores, axis=-1))
    expo = jnp.exp(scores - top_new[..., None])
    total_new = jnp.sum(expo, axis=-1)
    accum_new = jnp.einsum(
        "hqk,khd->hqd", expo.astype(jnp.bfloat16), value_rows, preferred_element_type=jnp.float32
    )
    attn = (accum_new / total_new[..., None]).astype(jnp.bfloat16)
    attn = attn.transpose(1, 0, 2).reshape(tok_rows, head_count * VDIM)
    block_f = lax.all_gather(attn, "tp", axis=1, tiled=True).astype(jnp.float32)
    scaled = (block_f * out_gain[None, :]).astype(jnp.bfloat16)
    product = jnp.dot(scaled, out_proj, preferred_element_type=jnp.float32)
    product, squares = (product, jnp.sum(block_f * block_f, axis=-1))
    mixed = (product * lax.rsqrt(squares / out_gain.shape[0] + EPS)[:, None]).astype(jnp.bfloat16)
    row_count = moe_input.shape[0]
    top_count = expert_ids.shape[1]
    local_experts = w_gate.shape[0]
    ep_count = lax.axis_size("ep")
    expert_count = local_experts * ep_count
    stream_f = moe_input.astype(jnp.float32)
    normed = (
        stream_f * lax.rsqrt(jnp.mean(stream_f * stream_f, axis=-1, keepdims=True) + EPS) * moe_gain
    ).astype(jnp.bfloat16)
    flat_ids = expert_ids.reshape(-1)
    onehot = (flat_ids[:, None] == jnp.arange(expert_count, dtype=jnp.int32)[None, :]).astype(
        jnp.int32
    )
    slot_rank = jnp.sum((jnp.cumsum(onehot, axis=0) - onehot) * onehot, axis=1)
    slot_index = flat_ids * CAP + slot_rank
    token_index = jnp.arange(row_count * top_count, dtype=jnp.int32) // top_count
    slot_token = jnp.zeros((expert_count * CAP,), jnp.int32).at[slot_index].set(token_index)
    slot_used = jnp.zeros((expert_count * CAP,), jnp.bool_).at[slot_index].set(True)
    outgoing = jnp.where(slot_used[:, None], normed[slot_token], jnp.zeros((), jnp.bfloat16))
    outgoing = outgoing.reshape(ep_count, local_experts, CAP, normed.shape[1])
    piece_width = normed.shape[1] // lax.axis_size("tp")
    my_columns = lax.dynamic_slice_in_dim(
        outgoing, lax.axis_index("tp") * piece_width, piece_width, 3
    )
    arrived_part = lax.all_to_all(my_columns, "ep", split_axis=0, concat_axis=0, tiled=True)
    piece = lax.all_gather(arrived_part, "tp", axis=3, tiled=True)
    gate_acc = jnp.einsum("secd,edf->secf", piece, w_gate, preferred_element_type=jnp.float32)
    upper_acc = jnp.einsum("secd,edf->secf", piece, w_up, preferred_element_type=jnp.float32)
    hidden = (jax.nn.silu(gate_acc) * upper_acc).astype(jnp.bfloat16)
    out_cols = w_down.shape[2] // lax.axis_size("tp")
    term = jnp.einsum("secf,efd->dsec", hidden, w_down, preferred_element_type=jnp.float32)
    summed = lax.psum_scatter(
        term.reshape(lax.axis_size("tp") * out_cols, -1).astype(jnp.bfloat16),
        "tp",
        scatter_dimension=0,
        tiled=True,
    )
    expert_y = summed.T.reshape(ep_count, local_experts * CAP, out_cols)
    returned_rows = lax.all_to_all(expert_y, "ep", split_axis=0, concat_axis=0, tiled=True).reshape(
        expert_count * CAP, out_cols
    )
    picked = returned_rows[slot_index].reshape(row_count, top_count, out_cols).astype(jnp.float32)
    expert_out = jnp.sum(picked * route_weights[..., None], axis=1).astype(jnp.bfloat16)
    return (mixed, expert_out)


def solution(mesh):
    in_specs = (
        P("ep", "tp"),
        P("ep", None),
        P("ep", None),
        P(),
        P(None, "tp"),
        P(None, "tp"),
        P(),
        P(),
        P(),
        P(None, "tp"),
        P("ep", None),
        P(),
        P("ep", None),
        P("ep", None),
        P("ep", None, "tp"),
        P("ep", None, "tp"),
        P("ep", "tp", None),
    )
    out_specs = (P("ep", "tp"), P("ep", "tp"))
    return jax.shard_map(shards, mesh=mesh, in_specs=in_specs, out_specs=out_specs, check_vma=False)
```

profile of v0, /device:TPU:0, one launch (start us, length us, event | category | flops | bytes accessed | tf_op | source)
XLA Modules:
  0.0 224.2 jit_solution(16331249084519766166)
XLA Ops:
  7.2 0.9 copy.35
  10.3 1.4 scatter_custom_fusion.1
  11.8 1.5 fusion.15
  13.3 1.6 fusion.17
  14.8 4.1 %gather_fusion = bf16[384,4096]{1,0:T(8,128)(2,1)} fusion(bf16[128,4096]{1,0:T(8,128)(2,1)S(1)} %fusion.17, s32[1024]{0:T(1024)S(1)} %pad_clamp_fusion.1), kind=kCustom, calls=%fused_computation | custom fusion | bytes 6292992 | tf_op jit(solution)/shard_map/gather | solution.py:147
  18.9 5.5 %gather.9 = bf16[8,4,12,4096]{3,2,1,0:T(8,128)(2,1)} reshape(bf16[384,4096]{1,0:T(8,128)(2,1)} %gather_fusion) | data formatting | bytes 6291456 | tf_op jit(solution)/shard_map/gather | solution.py:147
  24.4 1.5 scatter_custom_fusion
  26.0 1.5 dynamic-slice_select_fusion
  28.1 27.1 %all_to_all.10 = bf16[8,4,12,1024]{3,1,2,0:T(4,128)(2,1)S(1)} all-to-all(bf16[8,4,12,1024]{3,1,2,0:T(4,128)(2,1)S(1)} %copy.38), channel_id=1, replica_groups=mesh['ep'=8,'tp'=4] {'ep'}, dimensions={0} | all-to-all | bytes 1572864 | tf_op jit(solution)/shard_map/all_to_all | solution.py:153
  55.2 1.3 copy.39
  57.5 50.7 %all-gather.5.cloned.1.call-done = bf16[8,4,12,4096]{3,2,0,1:T(8,128)(2,1)} async-done(((bf16[8,4,12,1024]{3,2,0,1:T(8,128)(2,1)}), bf16[8,4,12,4096]{3,2,0,1:T(8,128)(2,1)}) %all-gather.5.cloned.1.call-update) | async-done | bytes 3145744 | tf_op jit(solution)/shard_map/all_gather | solution.py:154
  108.2 9.5 %fusion.21 = f32[8,4,12,512]{3,2,0,1:T(8,128)S(1)} fusion(bf16[8,4,12,4096]{3,2,0,1:T(8,128)(2,1)} %all-gather.5.cloned.1.call-done, bf16[4,4096,512]{2,1,0:T(8,128)(2,1)} %param.31), kind=kOutput, calls=%fused_computation.30 | convolution fusion | flops 1610612736 | bytes 20709376 | tf_op jit(solution)/shard_map/secd,edf->secf/dot_general | solution.py:155
  117.7 9.7 %fusion.30 = bf16[8,4,12,512]{3,2,0,1:T(8,128)(2,1)S(1)} fusion(bf16[8,4,12,4096]{3,2,0,1:T(8,128)(2,1)} %all-gather.5.cloned.1.call-done, bf16[4,4096,512]{2,1,0:T(8,128)(2,1)} %param.32, f32[8,4,12,512]{3,2,0,1:T(8,128)S(1)} %fusion.21), kind=kOutput, calls=%fused_computation.33 | convolution fusion | flops 1611792384 | bytes 21102592 | tf_op jit(solution)/shard_map/secd,edf->secf/dot_general | solution.py:156
  127.5 4.3 %fusion.9 = bf16[4096,8,4,12]{0,3,1,2:T(8,128)(2,1)} fusion(bf16[8,4,12,512]{3,2,0,1:T(8,128)(2,1)S(1)} %fusion.30, bf16[4,512,4096]{2,1,0:T(8,128)(2,1)S(1)} %bitcast.84), kind=kOutput, calls=%fused_computation.11 | convolution fusion | flops 1612185600 | bytes 20316160 | tf_op jit(solution)/shard_map/secf,efd->dsec/dot_general | solution.py:159
  131.8 4.6 %copy.40 = bf16[4096,8,4,12]{0,3,2,1:T(8,128)(2,1)} copy(bf16[4096,8,4,12]{0,3,1,2:T(8,128)(2,1)} %fusion.9) | data formatting | bytes 6291456 | tf_op jit(solution)/shard_map/convert_element_type | solution.py:161
  136.4 5.6 %convert_element_type.108 = bf16[4096,384]{0,1:T(8,128)(2,1)} reshape(bf16[4096,8,4,12]{0,3,2,1:T(8,128)(2,1)} %copy.40) | data formatting | bytes 6291456 | tf_op jit(solution)/shard_map/convert_element_type | solution.py:161
  142.1 0.8 copy-done.3
  144.0 12.8 %all_gather.13 = bf16[1024,32]{0,1:T(8,128)(2,1)S(1)} all-gather(bf16[128,32]{0,1:T(8,128)(2,1)S(1)} %copy-done.6), channel_id=1, replica_groups=mesh['ep'=8,'tp'=4] {'ep'}, dimensions={0}, use_global_device_ids=true | all-gather | bytes 73728 | tf_op jit(solution)/shard_map/all_gather | solution.py:102
  158.6 1.6 fusion.12
  160.8 2.6 %convolution_convert_fusion.1 = bf16[1024,256]{1,0:T(8,128)(2,1)} fusion(bf16[512,256]{1,0:T(8,128)(2,1)S(1)} %copy-done.13, bf16[1024,512]{1,0:T(8,128)(2,1)} %all-gather.3.cloned.1.call-done, f32[512]{0:T(512)S(1)} %copy-done.15, f32[1024]{0:T(1024)S(1)} %add_rsqrt_fusion.1), kind=kOutput, calls=%fused_computation.35 | convolution fusion | flops 270794752 | bytes 1841152 | tf_op jit(solution)/shard_map/dot_general | solution.py:58
  163.3 1.2 copy.33
  166.1 2.0 fusion.18
  168.0 18.2 %reduce-scatter.2.cloned.1.call-done = bf16[1024,384]{0,1:T(8,128)(2,1)} async-done(((bf16[4096,384]{0,1:T(8,128)(2,1)}), bf16[1024,384]{0,1:T(8,128)(2,1)}) %reduce-scatter.2.cloned.1.call-update) | async-done | bytes 786448 | tf_op jit(solution)/shard_map/reduce_scatter | solution.py:160
  186.2 4.6 %all-to-all-start.1 = ((bf16[8,48,1024]{2,1,0:T(8,128)(2,1)}), bf16[8,48,1024]{2,1,0:T(8,128)(2,1)S(1)}, u32[]{:S(2)}, u32[]{:S(2)}) async-start(bf16[8,48,1024]{2,1,0:T(8,128)(2,1)} %bitcast.89), calls=%async_computation.2 | async-start | bytes 1572864 | tf_op jit(solution)/shard_map/all_to_all | solution.py:167
  190.9 2.3 %fusion.19 = f32[4,128]{1,0:T(4,128)S(1)} fusion(f32[4,128,1024]{2,1,0:T(8,128)} %get-tuple-element.11, f32[4,128]{1,0:T(4,128)S(1)} %broadcast_maximum_fusion, pred[128,1024]{1,0:T(8,128)(4,1)S(1)} %iota_compare_fusion), kind=kLoop, calls=%fused_computation.25 | loop fusion | flops 2096640 | bytes 2232320 | tf_op jit(solution)/shard_map/reduce_sum | solution.py:118
  193.9 0.7 fusion.35
  194.7 8.9 %all_gather.14 = bf16[128,1024]{0,1:T(8,128)(2,1)S(1)} all-gather(bf16[128,256]{0,1:T(8,128)(2,1)S(1)} %bitcast.90), channel_id=1, replica_groups=mesh['ep'=8,'tp'=4] {'tp'}, dimensions={1}, use_global_device_ids=true | all-gather | bytes 327680 | tf_op jit(solution)/shard_map/all_gather | solution.py:124
  203.8 1.4 fusion.33
  205.2 6.6 %all-to-all-done.1 = bf16[8,48,1024]{2,1,0:T(8,128)(2,1)S(1)} async-done(((bf16[8,48,1024]{2,1,0:T(8,128)(2,1)}), bf16[8,48,1024]{2,1,0:T(8,128)(2,1)S(1)}, u32[]{:S(2)}, u32[]{:S(2)}) %all-to-all-start.1) | async-done | bytes 786464 | tf_op jit(solution)/shard_map/all_to_all | solution.py:167
  211.8 2.1 gather_fusion.1
  213.9 1.7 reshape.278
  215.6 2.1 multiply_reduce_fusion.1
  (94 shorter events, 9.7 us)
Async XLA Ops:
  7.2 196.6 %copy-start = (bf16[1024,1024]{1,0:T(8,128)(2,1)S(1)}, bf16[1024,1024]{1,0:T(8,128)(2,1)}, u32[]{:S(2)}) copy-start(bf16[1024,1024]{1,0:T(8,128)(2,1)} %param.26) | copy-start | bytes 6291460
  7.2 101.0 %all-gather.5.cloned.1.call-start = ((), (), s32[]{:S(2)}) async-start(), calls=%async_computation.4 | async-start | bytes 5242880 | tf_op jit(solution)/shard_map/all_gather | solution.py:154
  56.5 102.1 %all-gather.3.cloned.1.call-start = ((), (), s32[]{:S(2)}) async-start(), calls=%async_computation.3 | async-start | bytes 1179648 | tf_op jit(solution)/shard_map/all_gather | solution.py:101
  57.3 129.0 %reduce-scatter.2.cloned.1.call-start = ((), (), s32[]{:S(2)}) async-start(), calls=%async_computation.5 | async-start | bytes 3932160 | tf_op jit(solution)/shard_map/reduce_scatter | solution.py:160
  108.2 19.3 %slice-start = ((s8[16777216]{0:T(1024)(128)(4,1)}), s8[4194304]{0:T(1024)(128)(4,1)S(1)}, s32[]{:S(2)}) async-start(s8[16777216]{0:T(1024)(128)(4,1)} %bitcast.83), calls=%async_computation.6 | async-start | bytes 8388608
  108.2 19.3 %slice-start.1 = ((s8[16777216]{0:T(1024)(128)(4,1)}), s8[4194304]{0:T(1024)(128)(4,1)S(1)}, s32[]{:S(2)}) async-start(s8[16777216]{0:T(1024)(128)(4,1)} %bitcast.83), calls=%async_computation.7 | async-start | bytes 8388608
  117.7 9.8 %slice-start.2 = ((s8[16777216]{0:T(1024)(128)(4,1)}), s8[4194304]{0:T(1024)(128)(4,1)S(1)}, s32[]{:S(2)}) async-start(s8[16777216]{0:T(1024)(128)(4,1)} %bitcast.83), calls=%async_computation.8 | async-start | bytes 8388608
  117.7 9.8 %slice-start.3 = ((s8[16777216]{0:T(1024)(128)(4,1)}), s8[4194304]{0:T(1024)(128)(4,1)S(1)}, s32[]{:S(2)}) async-start(s8[16777216]{0:T(1024)(128)(4,1)} %bitcast.83), calls=%async_computation.9 | async-start | bytes 8388608
  142.0 0.9 copy-start.3
  142.0 1.1 copy-start.11
  142.0 1.8 copy-start.10
  142.0 1.9 copy-start.6
  142.1 18.7 %copy-start.13 = (bf16[512,256]{1,0:T(8,128)(2,1)S(1)}, bf16[512,256]{1,0:T(8,128)(2,1)}, u32[]{:S(2)}) copy-start(bf16[512,256]{1,0:T(8,128)(2,1)} %param.21) | copy-start | bytes 786436
  142.1 18.7 %copy-start.15 = (f32[512]{0:T(512)S(1)}, f32[512]{0:T(512)}, u32[]{:S(2)}) copy-start(f32[512]{0:T(512)} %param.20) | copy-start | bytes 6148
  160.2 0.6 copy-start.8
  164.6 0.7 copy-start.12
  165.2 0.8 copy-start.4
  165.2 0.8 copy-start.5
  168.0 25.1 %copy-start.9 = (f32[1024]{0:T(1024)S(1)}, f32[1024]{0:T(1024)}, u32[]{:S(2)}) copy-start(f32[1024]{0:T(1024)} %copy-done.8) | copy-start | bytes 12292
  168.0 25.1 %copy-start.14 = (bf16[512,256]{1,0:T(8,128)(2,1)S(1)}, bf16[512,256]{1,0:T(8,128)(2,1)}, u32[]{:S(2)}) copy-start(bf16[512,256]{1,0:T(8,128)(2,1)} %param.22) | copy-start | bytes 786436
  168.0 25.2 %copy-start.16 = (f32[512]{0:T(512)S(1)}, f32[512]{0:T(512)}, u32[]{:S(2)}) copy-start(f32[512]{0:T(512)} %param.20) | copy-start | bytes 6148
  186.2 25.6 %all-to-all-start.1 = ((bf16[8,48,1024]{2,1,0:T(8,128)(2,1)}), bf16[8,48,1024]{2,1,0:T(8,128)(2,1)S(1)}, u32[]{:S(2)}, u32[]{:S(2)}) async-start(bf16[8,48,1024]{2,1,0:T(8,128)(2,1)} %bitcast.89), calls=%async_computation.2 | async-start | bytes 1572864 | tf_op jit(solution)/shard_map/all_to_all | solution.py:167
  190.8 2.4 %copy-start.2 = (bf16[1024,512]{1,0:T(8,128)(2,1)S(1)}, bf16[1024,512]{1,0:T(8,128)(2,1)}, u32[]{:S(2)}) copy-start(bf16[1024,512]{1,0:T(8,128)(2,1)} %all-gather.3.cloned.1.call-done) | copy-start | bytes 3145732
  190.8 3.0 %copy-start.1 = (f32[4,128,1024]{2,1,0:T(8,128)S(1)}, f32[4,128,1024]{2,1,0:T(8,128)}, u32[]{:S(2)}) copy-start(f32[4,128,1024]{2,1,0:T(8,128)} %get-tuple-element.11) | copy-start | bytes 6291460
  193.9 9.9 %copy-start.7 = (f32[1024]{0:T(1024)S(1)}, f32[1024]{0:T(1024)}, u32[]{:S(2)}) copy-start(f32[1024]{0:T(1024)} %param.25) | copy-start | bytes 12292
Sparse Core Ops, SparseCore 0:
  56.6 51.4 all-gather.4
  109.8 22.2 all-gather.2
  142.2 43.9 reduce-scatter.1
where the time goes:
time: 225 us; the launch traced here: 224 us
  waiting for transfers between devices  76.2 us (34%)
  blocking collectives  48.8 us (22%)
  local copies, waits for them, and re-layouts  34.5 us (15%)
  matrix products  30.9 us (14%)
  other arithmetic  14.7 us (7%)
  between operations  14.2 us (6%)
  starting transfers between devices  4.91 us (2%)
    all_gather x1, waiting for transfers between devices, shards(): piece = lax.all_gather(arrived_part, 'tp', axis=3, tiled=True)  50.7 us
    all_to_all x1, blocking collectives, shards(): lax.all_to_all(my_columns, 'ep', split_axis=0, concat_axis=0, tiled=True)  27.1 us
    reduce_scatter x1, waiting for transfers between devices, shards(): lax.psum_scatter(term.reshape(lax.axis_size('tp') * out_cols, -1).astype(...  18.2 us
    all_gather x1, blocking collectives, shards(): lax.all_gather(rope_key, 'ep', axis=0, tiled=True)  12.8 us
    convert_element_type x2, local copies, waits for them, and re-layouts, shards(): term.reshape(lax.axis_size('tp') * out_cols, -1).astype(jnp.bfloat16)  10.2 us
    dot_general x1, matrix products, shards(): jnp.einsum('secd,edf->secf', piece, w_up, preferred_element_type=jnp.floa...  9.73 us
    gather x2, local copies, waits for them, and re-layouts, shards(): normed[slot_token]  9.56 us
    dot_general x1, matrix products, shards(): jnp.einsum('secd,edf->secf', piece, w_gate, preferred_element_type=jnp.fl...  9.51 us
  transfers between devices with their start and end apart: 4, of which 3 were waited for; matrix products, arithmetic and copies ran while one was open for 22% of the time, Pallas kernels for 0%

commit v1 on v0

--- a/solution.py
+++ b/solution.py
@@ -1,6 +1,10 @@
+import functools
+
 import jax
 import jax.numpy as jnp
 from jax import lax
+from jax.experimental import pallas as pl
+from jax.experimental.pallas import tpu as pltpu
 from jax.sharding import PartitionSpec as P
 
 NOPE = 64
@@ -172,6 +176,560 @@
     return (mixed, expert_out)
 
 
+MESH = pl.DeviceIdType.MESH
+GROUP = 8
+PAD = 128
+
+
+def group_cap():
+    return GROUP * CAP // 2
+
+
+def rdma(src, dst, send_sem, recv_sem, device):
+    copy = pltpu.make_async_remote_copy(
+        src_ref=src,
+        dst_ref=dst,
+        send_sem=send_sem,
+        recv_sem=recv_sem,
+        device_id=device,
+        device_id_type=MESH,
+    )
+    copy.start()
+    return copy
+
+
+def arrived(dst, sem, device):
+    pltpu.make_async_remote_copy(
+        src_ref=dst,
+        dst_ref=dst,
+        send_sem=sem,
+        recv_sem=sem,
+        device_id=device,
+        device_id_type=MESH,
+    ).wait_recv()
+
+
+def places(planes):
+    ep = lax.axis_index("ep")
+    tp = lax.axis_index("tp")
+    plane = ep // 2
+    core = ep % 2
+
+    def along(offset):
+        return (lax.rem(plane + offset + planes, planes) * 2 + core, tp)
+
+    partner = (plane * 2 + 1 - core, tp)
+    near_x = (ep, tp ^ 1)
+    near_y = (ep, tp ^ 2)
+    corner = (ep, tp ^ 3)
+    return tp, along, partner, near_x, near_y, corner
+
+
+def greet(peers):
+    barrier = pltpu.get_barrier_semaphore()
+    for peer in peers:
+        pl.semaphore_signal(barrier, inc=1, device_id=peer, device_id_type=MESH)
+    pl.semaphore_wait(barrier, len(peers))
+
+
+def dispatch_kernel(
+    planes,
+    out_ref,
+    meta_ref,
+    kv_ref,
+    rows_ref,
+    metas_ref,
+    keys_ref,
+    zs,
+    zr,
+    xs,
+    xr,
+    ps,
+    pr,
+    loc,
+):
+    tp, along, partner, near_x, near_y, _ = places(planes)
+    greet([along(d) for d in range(1, planes)] + [partner, near_x, near_y])
+    half_w = out_ref.shape[2] // 2
+    half_r = kv_ref.shape[0] // 2
+    sent = []
+    local = [
+        pltpu.make_async_copy(kv_ref, keys_ref.at[tp, 0, 0], loc.at[0]),
+        pltpu.make_async_copy(meta_ref.at[0], metas_ref.at[0, 0], loc.at[1]),
+        pltpu.make_async_copy(out_ref.at[0], rows_ref.at[tp, 0, 0], loc.at[2]),
+    ]
+    for copy in local:
+        copy.start()
+    for d in range(1, planes):
+        sent.append(rdma(kv_ref, keys_ref.at[tp, 0, d], zs.at[0, d], zr.at[0, d], along(d)))
+    for d in range(1, planes):
+        sent.append(
+            rdma(meta_ref.at[d], metas_ref.at[0, d], zs.at[1, d], zr.at[1, d], along(d))
+        )
+        sent.append(
+            rdma(out_ref.at[d], rows_ref.at[tp, 0, d], zs.at[2, d], zr.at[2, d], along(d))
+        )
+    for copy in local:
+        copy.wait()
+    bufs = (keys_ref, rows_ref)
+
+    def halves(kind, ref):
+        if kind == 0:
+            return ref.at[pl.ds(0, half_r)], ref.at[pl.ds(half_r, half_r)]
+        return ref.at[:, pl.ds(0, half_w)], ref.at[:, pl.ds(half_w, half_w)]
+
+    def to_partner(kind, which, q, d):
+        sent.append(
+            rdma(
+                bufs[kind].at[q, 0, d],
+                bufs[kind].at[q, 1, d],
+                ps.at[kind, which, d],
+                pr.at[kind, which, d],
+                partner,
+            )
+        )
+
+    def first(kind, d):
+        mine = bufs[kind].at[tp, 0, d]
+        if d > 0:
+            arrived(mine, zr.at[2 * kind, d], along(-d))
+        sent.append(rdma(mine, mine, xs.at[kind, 0, d], xr.at[kind, 0, d], near_x))
+        sent.append(rdma(mine, mine, xs.at[kind, 1, d], xr.at[kind, 1, d], near_y))
+        to_partner(kind, 0, tp, d)
+        if kind == 1:
+            part = metas_ref.at[0, d]
+            if d > 0:
+                arrived(part, zr.at[1, d], along(-d))
+            sent.append(rdma(part, metas_ref.at[1, d], ps.at[2, 0, d], pr.at[2, 0, d], partner))
+
+    def second(kind, d):
+        from_x = bufs[kind].at[tp ^ 1, 0, d]
+        arrived(from_x, xr.at[kind, 0, d], near_x)
+        low, _ = halves(kind, from_x)
+        sent.append(rdma(low, low, xs.at[kind, 2, d], xr.at[kind, 2, d], near_y))
+        from_y = bufs[kind].at[tp ^ 2, 0, d]
+        arrived(from_y, xr.at[kind, 1, d], near_y)
+        _, high = halves(kind, from_y)
+        sent.append(rdma(high, high, xs.at[kind, 3, d], xr.at[kind, 3, d], near_x))
+        to_partner(kind, 1, tp ^ 1, d)
+        to_partner(kind, 2, tp ^ 2, d)
+
+    def third(kind, d):
+        low, high = halves(kind, bufs[kind].at[tp ^ 3, 0, d])
+        arrived(low, xr.at[kind, 2, d], near_y)
+        arrived(high, xr.at[kind, 3, d], near_x)
+        to_partner(kind, 3, tp ^ 3, d)
+
+    jobs = [(0, d) for d in range(planes)] + [(1, d) for d in range(planes)]
+    for step in range(len(jobs) + 4):
+        if step < len(jobs):
+            first(*jobs[step])
+        if 0 <= step - 2 < len(jobs):
+            second(*jobs[step - 2])
+        if 0 <= step - 4 < len(jobs):
+            third(*jobs[step - 4])
+    for d in range(planes):
+        for kind in range(2):
+            for which, flip in enumerate((0, 1, 2, 3)):
+                arrived(bufs[kind].at[tp ^ flip, 1, d], pr.at[kind, which, d], partner)
+        arrived(metas_ref.at[1, d], pr.at[2, 0, d], partner)
+    for copy in sent:
+        copy.wait_send()
+
+
+def dispatch(outgoing, metas, kv_part, tp_count):
+    planes, cap, width = outgoing.shape
+    dma = pltpu.SemaphoreType.DMA
+    return pl.pallas_call(
+        functools.partial(dispatch_kernel, planes),
+        out_shape=(
+            jax.ShapeDtypeStruct((tp_count, 2, planes, cap, width), jnp.bfloat16),
+            jax.ShapeDtypeStruct((2, planes, cap, PAD), jnp.bfloat16),
+            jax.ShapeDtypeStruct((tp_count, 2, planes) + kv_part.shape, jnp.bfloat16),
+        ),
+        in_specs=[pl.BlockSpec(memory_space=pltpu.VMEM)] * 3,
+        out_specs=(pl.BlockSpec(memory_space=pltpu.VMEM),) * 3,
+        scratch_shapes=[
+            dma((3, planes)),
+            dma((3, planes)),
+            dma((2, 4, planes)),
+            dma((2, 4, planes)),
+            dma((3, 4, planes)),
+            dma((3, 4, planes)),
+            dma((3,)),
+        ],
+        compiler_params=pltpu.CompilerParams(
+            collective_id=0, has_side_effects=True, vmem_limit_bytes=40 * 2**20
+        ),
+        name="dispatch",
+    )(outgoing, metas, kv_part)
+
+
+def expert_kernel(
+    pick_ref, place_ref, weight_ref, rows_ref, gate_ref, up_ref, down_ref, out_ref, g_acc, u_acc, total
+):
+    expert = pl.program_id(0)
+    quarter = pl.program_id(1)
+    experts = pl.num_programs(0)
+    quarters = pl.num_programs(1)
+
+    picked = jnp.dot(
+        pick_ref[...], rows_ref[quarter], preferred_element_type=jnp.float32
+    ).astype(jnp.bfloat16)
+    gate = jnp.dot(picked, gate_ref[...], preferred_element_type=jnp.float32)
+    upper = jnp.dot(picked, up_ref[...], preferred_element_type=jnp.float32)
+
+    @pl.when(quarter == 0)
+    def _():
+        g_acc[...] = gate
+        u_acc[...] = upper
+
+    @pl.when(quarter > 0)
+    def _():
+        g_acc[...] += gate
+        u_acc[...] += upper
+
+    @pl.when(quarter == quarters - 1)
+    def _():
+        g = g_acc[...]
+        hidden = (g / (1.0 + jnp.exp(-g)) * u_acc[...] * weight_ref[...]).astype(jnp.bfloat16)
+        blocks, parts, cap, width = out_ref.shape
+        for q in range(parts):
+            y = jnp.dot(
+                hidden, down_ref[:, q * width : (q + 1) * width], preferred_element_type=jnp.float32
+            ).astype(jnp.bfloat16)
+            back = jnp.dot(place_ref[...], y, preferred_element_type=jnp.float32)
+
+            @pl.when(expert == 0)
+            def _():
+                total[q] = back
+
+            @pl.when(expert > 0)
+            def _():
+                total[q] += back
+
+            @pl.when(expert == experts - 1)
+            def _():
+                out_ref[:, q] = total[q].reshape(blocks, cap, width).astype(jnp.bfloat16)
+
+
+def run_experts(pick, place, weights, rows, w_gate, w_up, w_down, blocks, cap):
+    experts, slots, row_count = pick.shape
+    parts, _, width = rows.shape
+    hidden = w_gate.shape[2]
+    return pl.pallas_call(
+        expert_kernel,
+        grid=(experts, parts),
+        out_shape=jax.ShapeDtypeStruct((blocks, parts, cap, width), jnp.bfloat16),
+        in_specs=[
+            pl.BlockSpec((None, slots, row_count), lambda e, q: (e, 0, 0)),
+            pl.BlockSpec((None, row_count, slots), lambda e, q: (e, 0, 0)),
+            pl.BlockSpec((None, slots, 1), lambda e, q: (e, 0, 0)),
+            pl.BlockSpec((parts, row_count, width), lambda e, q: (0, 0, 0)),
+            pl.BlockSpec((None, width, hidden), lambda e, q: (e, q, 0)),
+            pl.BlockSpec((None, width, hidden), lambda e, q: (e, q, 0)),
+            pl.BlockSpec((None, hidden, parts * width), lambda e, q: (e, 0, 0)),
+        ],
+        out_specs=pl.BlockSpec((blocks, parts, cap, width), lambda e, q: (0, 0, 0, 0)),
+        scratch_shapes=[
+            pltpu.VMEM((slots, hidden), jnp.float32),
+            pltpu.VMEM((slots, hidden), jnp.float32),
+            pltpu.VMEM((parts, row_count, width), jnp.float32),
+        ],
+        compiler_params=pltpu.CompilerParams(
+            dimension_semantics=("arbitrary", "arbitrary"), vmem_limit_bytes=56 * 2**20
+        ),
+        name="experts",
+    )(pick, place, weights, rows, w_gate, w_up, w_down)
+
+
+def combine_kernel(
+    planes,
+    part_ref,
+    attn_ref,
+    back_ref,
+    heads_ref,
+    other,
+    sums,
+    bx1,
+    by1,
+    bx2,
+    by2,
+    done,
+    as_,
+    ar,
+    ps,
+    pr,
+    xs,
+    xr,
+    zs,
+    zr,
+    loc,
+):
+    tp, along, partner, near_x, near_y, corner = places(planes)
+    greet([along(d) for d in range(1, planes)] + [partner, near_x, near_y, corner])
+    half_w = part_ref.shape[4] // 2
+    low, high = pl.ds(0, half_w), pl.ds(half_w, half_w)
+    sent = []
+    order = list(range(1, planes)) + [0]
+    for d in order:
+        sent.append(rdma(part_ref.at[1, d], other.at[d], ps.at[d], pr.at[d], partner))
+    own = pltpu.make_async_copy(attn_ref, heads_ref.at[tp], loc.at[0])
+    own.start()
+    for i, peer in enumerate((near_x, near_y, corner)):
+        sent.append(rdma(attn_ref, heads_ref.at[tp], as_.at[i], ar.at[i], peer))
+
+    def first(d):
+        arrived(other.at[d], pr.at[d], partner)
+        for q in range(part_ref.shape[2]):
+            sums[d, q] = (
+                part_ref[0, d, q].astype(jnp.float32) + other[d, q].astype(jnp.float32)
+            ).astype(jnp.bfloat16)
+        piece = sums.at[d, tp ^ 3]
+        sent.append(rdma(piece.at[:, low], bx1.at[d], xs.at[0, d], xr.at[0, d], near_x))
+        sent.append(rdma(piece.at[:, high], by1.at[d], xs.at[1, d], xr.at[1, d], near_y))
+
+    def second(d):
+        arrived(bx1.at[d], xr.at[0, d], near_x)
+        sums[d, tp ^ 2, :, low] = (
+            sums[d, tp ^ 2, :, low].astype(jnp.float32) + bx1[d].astype(jnp.float32)
+        ).astype(jnp.bfloat16)
+        sent.append(rdma(sums.at[d, tp ^ 2], by2.at[d], xs.at[3, d], xr.at[3, d], near_y))
+        arrived(by1.at[d], xr.at[1, d], near_y)
+        sums[d, tp ^ 1, :, high] = (
+            sums[d, tp ^ 1, :, high].astype(jnp.float32) + by1[d].astype(jnp.float32)
+        ).astype(jnp.bfloat16)
+        sent.append(rdma(sums.at[d, tp ^ 1], bx2.at[d], xs.at[2, d], xr.at[2, d], near_x))
+
+    def third(d):
+        arrived(bx2.at[d], xr.at[2, d], near_x)
+        arrived(by2.at[d], xr.at[3, d], near_y)
+        full = (
+            sums[d, tp].astype(jnp.float32)
+            + bx2[d].astype(jnp.float32)
+            + by2[d].astype(jnp.float32)
+        ).astype(jnp.bfloat16)
+        if d == 0:
+            back_ref[0] = full
+        else:
+            done[d] = full
+            sent.append(rdma(done.at[d], back_ref.at[d], zs.at[d], zr.at[d], along(-d)))
+
+    for step in range(planes + 2):
+        if step < planes:
+            first(order[step])
+        if 0 <= step - 1 < planes:
+            second(order[step - 1])
+        if 0 <= step - 2 < planes:
+            third(order[step - 2])
+    own.wait()
+    for i, peer in enumerate((near_x, near_y, corner)):
+        arrived(heads_ref.at[tp ^ (i + 1)], ar.at[i], peer)
+    for d in range(1, planes):
+        arrived(back_ref.at[d], zr.at[d], along(d))
+    for copy in sent:
+        copy.wait_send()
+
+
+def combine(parts, attn):
+    _, planes, tp_count, cap, width = parts.shape
+    dma = pltpu.SemaphoreType.DMA
+    bf = jnp.bfloat16
+    return pl.pallas_call(
+        functools.partial(combine_kernel, planes),
+        out_shape=(
+            jax.ShapeDtypeStruct((planes, cap, width), bf),
+            jax.ShapeDtypeStruct((tp_count,) + attn.shape, bf),
+        ),
+        in_specs=[pl.BlockSpec(memory_space=pltpu.VMEM)] * 2,
+        out_specs=(pl.BlockSpec(memory_space=pltpu.VMEM),) * 2,
+        scratch_shapes=[
+            pltpu.VMEM((planes, tp_count, cap, width), bf),
+            pltpu.VMEM((planes, tp_count, cap, width), bf),
+            pltpu.VMEM((planes, cap, width // 2), bf),
+            pltpu.VMEM((planes, cap, width // 2), bf),
+            pltpu.VMEM((planes, cap, width), bf),
+            pltpu.VMEM((planes, cap, width), bf),
+            pltpu.VMEM((planes, cap, width), bf),
+            dma((3,)),
+            dma((3,)),
+            dma((planes,)),
+            dma((planes,)),
+            dma((4, planes)),
+            dma((4, planes)),
+            dma((planes,)),
+            dma((planes,)),
+            dma((1,)),
+        ],
+        compiler_params=pltpu.CompilerParams(
+            collective_id=1, has_side_effects=True, vmem_limit_bytes=40 * 2**20
+        ),
+        name="combine",
+    )(parts, attn)
+
+
+def grouped_shards(
+    queries,
+    kv_latent,
+    rope_key,
+    latent_gain,
+    key_up,
+    value_up,
+    query_gain,
+    key_gain,
+    out_gain,
+    out_proj,
+    moe_input,
+    moe_gain,
+    expert_ids,
+    route_weights,
+    w_gate,
+    w_up,
+    w_down,
+):
+    f32, bf = jnp.float32, jnp.bfloat16
+    ep, tp = lax.axis_index("ep"), lax.axis_index("tp")
+    tp_count = lax.axis_size("tp")
+    planes = lax.axis_size("ep") // 2
+    plane, core = ep // 2, ep % 2
+    tokens, model = moe_input.shape
+    width = model // tp_count
+    local_experts = w_gate.shape[0]
+    cap = group_cap()
+    blocks = 2 * planes
+
+    group = expert_ids[:, 0] // GROUP
+    offset = lax.rem(group - plane + planes, planes)
+    before = (jnp.arange(tokens)[:, None] > jnp.arange(tokens)[None, :]).astype(bf)
+    in_group = offset[:, None] == jnp.arange(planes)[None, :]
+    local_ids = expert_ids % GROUP
+    hit = [offset[:, None] * GROUP + local_ids[:, k : k + 1] == jnp.arange(planes * GROUP)[None, :] for k in range(2)]
+    counted = jnp.concatenate([in_group, hit[0] | hit[1]], axis=1).astype(bf)
+    earlier = jnp.dot(before, counted, preferred_element_type=f32)
+    rank = jnp.sum(jnp.where(in_group, earlier[:, :planes], 0.0), axis=1).astype(jnp.int32)
+    codes = [
+        local_ids[:, k].astype(f32) * CAP
+        + jnp.sum(jnp.where(hit[k], earlier[:, planes:], 0.0), axis=1)
+        + 1.0
+        for k in range(2)
+    ]
+    weight_high = lax.reduce_precision(route_weights, 8, 7)
+    weight_low = route_weights - weight_high
+    meta = jnp.concatenate(
+        [codes[0][:, None], codes[1][:, None], weight_high, weight_low], axis=1
+    ).astype(bf)
+    meta = jnp.pad(meta, ((0, 0), (0, PAD - meta.shape[1])))
+    slot = offset * cap + rank
+    select = (jnp.arange(planes * cap)[:, None] == slot[None, :]).astype(bf)
+
+    stream_f = moe_input.astype(f32)
+    scale = lax.rsqrt(jnp.mean(stream_f * stream_f, axis=-1, keepdims=True) + EPS)
+    own_cols = lax.dynamic_slice_in_dim(moe_input, tp * width, width, 1).astype(f32)
+    own_gain = lax.dynamic_slice_in_dim(moe_gain, tp * width, width, 0)
+    normed = (own_cols * scale * own_gain).astype(bf)
+    outgoing = jnp.dot(select, normed, preferred_element_type=f32).astype(bf)
+    metas_out = jnp.dot(select, meta, preferred_element_type=f32).astype(bf)
+
+    kv_rows = kv_latent.shape[0] // tp_count
+    kv_all = jnp.pad(
+        jnp.concatenate([kv_latent, rope_key], axis=1), ((0, 0), (0, PAD - ROPE))
+    )
+    kv_part = lax.dynamic_slice_in_dim(kv_all, tp * kv_rows, kv_rows, 0)
+    rows, metas, keys = dispatch(
+        outgoing.reshape(planes, cap, width), metas_out.reshape(planes, cap, PAD), kv_part, tp_count
+    )
+
+    row_total = blocks * cap
+    slots = blocks * CAP
+    info = metas.reshape(row_total, PAD)[:, :6].astype(f32)
+    block_of = jnp.arange(row_total, dtype=jnp.int32) // cap
+    positions = []
+    for k in range(2):
+        code = info[:, k].astype(jnp.int32) - 1 - core * (local_experts * CAP)
+        inside = (info[:, k] > 0.5) & (code >= 0) & (code < local_experts * CAP)
+        where = (code // CAP) * slots + block_of * CAP + code % CAP
+        positions.append(jnp.where(inside, where, -1))
+    slot_ids = jnp.arange(local_experts * slots, dtype=jnp.int32).reshape(local_experts, slots)
+    match = [slot_ids[:, :, None] == positions[k][None, None, :] for k in range(2)]
+    pick = (match[0] | match[1]).astype(bf)
+    flip = [slot_ids[:, None, :] == positions[k][None, :, None] for k in range(2)]
+    place = (flip[0] | flip[1]).astype(bf)
+    weight_of = [info[:, 2 + k] + info[:, 4 + k] for k in range(2)]
+    weights = jnp.sum(
+        jnp.where(match[0], weight_of[0][None, None, :], 0.0)
+        + jnp.where(match[1], weight_of[1][None, None, :], 0.0),
+        axis=2,
+        keepdims=True,
+    )
+    partial = run_experts(
+        pick,
+        place,
+        weights,
+        rows.reshape(tp_count, row_total, width),
+        w_gate,
+        w_up,
+        w_down,
+        blocks,
+        cap,
+    ).reshape(2, planes, tp_count, cap, width)
+
+    tok_rows = queries.shape[0]
+    head_count = key_up.shape[1] // NOPE
+    query_pos = ep * tok_rows + jnp.arange(tok_rows, dtype=jnp.int32)
+    query_rot = make_queries(queries, query_gain, query_pos)
+    latent_width = kv_latent.shape[1]
+    key_table = keys.reshape(-1, keys.shape[-1])
+    quarter = jnp.arange(tp_count, dtype=jnp.int32)[:, None, None, None]
+    parity = jnp.arange(2, dtype=jnp.int32)[None, :, None, None]
+    away = jnp.arange(planes, dtype=jnp.int32)[None, None, :, None]
+    key_block = lax.rem(plane - away + planes, planes) * 2 + lax.rem(core + parity, 2)
+    key_pos = (
+        key_block * tok_rows
+        + quarter * kv_rows
+        + jnp.arange(kv_rows, dtype=jnp.int32)[None, None, None, :]
+    ).reshape(-1)
+    key_rot, value_rows = make_keys(
+        key_table[:, :latent_width],
+        key_table[:, latent_width : latent_width + ROPE],
+        latent_gain,
+        key_up,
+        value_up,
+        key_gain,
+        key_pos,
+    )
+    scores = (
+        jnp.einsum("qhd,khd->hqk", query_rot, key_rot, preferred_element_type=f32) * QKD ** (-0.5)
+    )
+    visible = key_pos[None, :] <= query_pos[:, None]
+    scores = jnp.where(visible[None], scores, -1e30)
+    expo = jnp.exp(scores - jnp.max(scores, axis=-1, keepdims=True))
+    total = jnp.sum(expo, axis=-1)
+    accum = jnp.einsum("hqk,khd->hqd", expo.astype(bf), value_rows, preferred_element_type=f32)
+    attn = (accum / total[..., None]).astype(bf)
+    attn = attn.transpose(1, 0, 2).reshape(tok_rows, head_count * VDIM)
+
+    returned, heads = combine(partial, attn)
+
+    block_f = heads.transpose(1, 0, 2).reshape(tok_rows, -1).astype(f32)
+    scaled = (block_f * out_gain[None, :]).astype(bf)
+    product = jnp.dot(scaled, out_proj, preferred_element_type=f32)
+    squares = jnp.sum(block_f * block_f, axis=-1)
+    mixed = (product * lax.rsqrt(squares / out_gain.shape[0] + EPS)[:, None]).astype(bf)
+    expert_out = lax.dot_general(
+        select,
+        returned.reshape(planes * cap, width),
+        (((0,), (0,)), ((), ())),
+        preferred_element_type=f32,
+    ).astype(bf)
+    return (mixed, expert_out)
+
+
+def layer(*arrays):
+    local_experts = arrays[14].shape[0]
+    fits = lax.axis_size("tp") == 4 and 2 * local_experts == GROUP
+    return grouped_shards(*arrays) if fits else shards(*arrays)
+
+
 def solution(mesh):
     in_specs = (
         P("ep", "tp"),
@@ -193,4 +751,4 @@
         P("ep", "tp", None),
     )
     out_specs = (P("ep", "tp"), P("ep", "tp"))
-    return jax.shard_map(shards, mesh=mesh, in_specs=in_specs, out_specs=out_specs, check_vma=False)
+    return jax.shard_map(layer, mesh=mesh, in_specs=in_specs, out_specs=out_specs, check_vma=False)

time: 225 us -> 126 us (0.56)
  Pallas kernels: 0 us -> 92.5 us
  waiting for transfers between devices: 76.2 us -> 0 us
  blocking collectives: 48.8 us -> 0 us
  matrix products: 30.9 us -> 7.09 us
  local copies, waits for them, and re-layouts: 34.5 us -> 13.5 us
  between operations: 14.2 us -> 1.09 us
  starting transfers between devices: 4.91 us -> 0 us
  other arithmetic: 14.7 us -> 11.5 us
    pallas_call x0 -> x3, Pallas kernels: none -> 92.5 us  [the longest x1 34.6 us: run_experts(): pl.pallas_call(expert_kernel, grid=(experts, parts), out_shape=jax.ShapeD...]
    all_gather x2 -> x0, waiting for transfers between devices: 50.7 us -> none  [the longest x1 50.7 us: shards(): piece = lax.all_gather(arrived_part, 'tp', axis=3, tiled=True)]
    all_to_all x1 -> x0, blocking collectives: 27.1 us -> none  [shards(): lax.all_to_all(my_columns, 'ep', split_axis=0, concat_axis=0, tiled=True)]
    dot_general x6 -> x7, matrix products: 27.7 us -> 5.14 us  [the longest x1 1.29 us: grouped_shards(): outgoing = jnp.dot(select, normed, preferred_element_type=f32).astype(bf)]
    all_gather x2 -> x0, blocking collectives: 21.7 us -> none  [the longest x1 12.8 us: shards(): lax.all_gather(rope_key, 'ep', axis=0, tiled=True)]
    reduce_scatter x1 -> x0, waiting for transfers between devices: 18.2 us -> none  [shards(): lax.psum_scatter(term.reshape(lax.axis_size('tp') * out_cols, -1).astype(...]
    gather x3 -> x0, local copies, waits for them, and re-layouts: 11.7 us -> none  [the longest x2 9.56 us: shards(): normed[slot_token]]
    convert_element_type x3 -> x1, local copies, waits for them, and re-layouts: 11.9 us -> 1.23 us  [grouped_shards(): block_f = heads.transpose(1, 0, 2).reshape(tok_rows, -1).astype(f32)]
  transfers between devices with their start and end apart: 4 -> 0, of which waited for: 3 -> 0; matrix products, arithmetic and copies ran while one was open for 22% -> 0% of each run, Pallas kernels for 0% -> 0%
where the time goes in v1:
time: 126 us
  Pallas kernels  92.5 us (73%)
  local copies, waits for them, and re-layouts  13.5 us (11%)
  other arithmetic  11.5 us (9%)
  matrix products  7.09 us (6%)
    pallas_call x1, Pallas kernels, run_experts(): pl.pallas_call(expert_kernel, grid=(experts, parts), out_shape=jax.ShapeD...  34.6 us
    pallas_call x1, Pallas kernels, dispatch(): pl.pallas_call(functools.partial(dispatch_kernel, planes), out_shape=(jax...  33.4 us
    pallas_call x1, Pallas kernels, combine(): pl.pallas_call(functools.partial(combine_kernel, planes), out_shape=(jax....  24.5 us
    unnamed x33, local copies, waits for them, and re-layouts  7.24 us

profile of v1, /device:TPU:0, one launch (start us, length us, event | category | flops | bytes accessed | tf_op | source)
XLA Modules:
  0.0 125.6 jit_solution(12095410888502449926)
XLA Ops:
  0.7 0.8 and_select_fusion
  1.5 0.7 add_bitcast_fusion.1
  2.5 0.7 fusion.82
  3.2 0.7 reduce-precision_convert_fusion
  4.0 0.7 dynamic_slice.10
  4.7 1.5 %multiply_reduce_fusion = f32[128]{0:T(128)S(1)} fusion(bf16[128,4096]{1,0:T(8,128)(2,1)} %param.27), kind=kLoop, calls=%fused_computation.7 | loop fusion | flops 1572736 | bytes 1049088 | tf_op jit(solution)/shard_map/reduce_sum | solution.py:626
  6.2 1.3 %convolution_convert_fusion.2 = bf16[192,1024]{1,0:T(8,128)(2,1)S(1)} fusion(f32[1024]{0:T(1024)S(1)} %dynamic_slice.10, f32[128]{0:T(128)S(1)} %add_rsqrt_fusion.4, bf16[128,4096]{1,0:T(8,128)(2,1)} %param.27, s32[]{:T(128)S(6)} %select_n.156, s32[128]{0:T(128)S(1)} %fusion.82), kind=kOutput, calls=%fused_computation.16 | convolution fusion | flops 51077120 | bytes 660484 | tf_op jit(solution)/shard_map/dot_general | solution.py:630
  7.7 33.4 %dispatch.1 = (bf16[4,2,4,48,1024]{4,3,2,1,0:T(8,128)(2,1)S(1)}, bf16[2,4,48,128]{3,2,1,0:T(8,128)(2,1)S(1)}, bf16[4,2,4,32,640]{4,3,2,1,0:T(8,128)(2,1)S(1)}) custom-call(bf16[4,48,1024]{2,1,0:T(8,128)(2,1)S(1)} %bitcast.61, bf16[4,48,128]{2,1,0:T(8,128)(2,1)S(1)} %bitcast.68, bf16[32,640]{1,0:T(8,128)(2,1)S(1)} %fusion.44.kv_ref), custom_call_target="tpu_custom_call" | custom-call | tf_op jit(solution)/shard_map/dispatch/pallas_call | solution.py:343
  41.2 1.7 %copy-done.2 = bf16[4,2,4,48,1024]{4,3,2,1,0:T(8,128)(2,1)} copy-done((bf16[4,2,4,48,1024]{4,3,2,1,0:T(8,128)(2,1)}, bf16[4,2,4,48,1024]{4,3,2,1,0:T(8,128)(2,1)S(1)}, u32[]{:S(2)}) %copy-start.2) | copy-done | bytes 3145752
  43.1 0.8 copy-done.3
  43.9 1.3 %convolution_convert_fusion.1 = bf16[1024,256]{1,0:T(8,128)(2,1)} fusion(bf16[512,256]{1,0:T(8,128)(2,1)S(1)} %copy-done.12, f32[512]{0:T(512)S(1)} %copy-done.14, f32[1024]{0:T(1024)S(1)} %add_rsqrt_fusion.1, bf16[1024,640]{1,0:T(8,128)(2,1)S(1)} %bitcast.63), kind=kOutput, calls=%fused_computation.15 | convolution fusion | flops 270794752 | bytes 1841152 | tf_op jit(solution)/shard_map/dot_general | solution.py:62
  45.2 1.3 %copy.36 = f32[1024,256]{0,1:T(8,128)S(1)} copy(bf16[1024,256]{1,0:T(8,128)(2,1)} %convolution_convert_fusion.1) | data formatting | bytes 1572864 | tf_op jit(solution)/shard_map/reshape | solution.py:71
  46.5 1.0 slice.106
  47.4 0.8 copy.41
  48.2 0.9 broadcast_in_dim.49
  49.7 1.1 copy-done.5
  51.6 1.1 subtract_convert_fusion
  53.3 0.7 fusion.3
  54.0 0.6 fusion.4
  54.6 0.7 copy-done.4
  55.3 0.7 convolution_convert_fusion
  56.0 0.7 fusion.8
  57.4 0.8 copy.34.weight_ref
  58.2 0.9 or_convert_fusion.place_ref
  59.2 0.9 fusion.21.pick_ref
  60.0 34.6 %experts.1 = bf16[8,4,48,1024]{3,2,1,0:T(8,128)(2,1)} custom-call(bf16[4,96,384]{2,1,0:T(8,128)(2,1)} %fusion.21.pick_ref, bf16[4,384,96]{2,1,0:T(8,128)(2,1)} %or_convert_fusion.place_ref, f32[4,96,1]{2,1,0:T(8,128)} %copy.34.weight_ref, bf16[4,384,1024]{2,1,0:T(8,128)(2,1)} %bitcast.60, bf16[4,4096,512]{2,1,0:T(8,128)(2,1)} %gate_ref.1, ...), custom_call_target="tpu_custom_call" | custom-call | tf_op jit(solution)/shard_map/experts/pallas_call | solution.py:420
  94.7 1.9 %copy-done.1 = bf16[8,4,48,1024]{3,2,1,0:T(8,128)(2,1)S(1)} copy-done((bf16[8,4,48,1024]{3,2,1,0:T(8,128)(2,1)S(1)}, bf16[8,4,48,1024]{3,2,1,0:T(8,128)(2,1)}, u32[]{:S(2)}) %copy-start.1) | copy-done | bytes 3145752
  96.6 24.5 %combine.1 = (bf16[4,48,1024]{2,1,0:T(8,128)(2,1)S(1)}, bf16[4,128,256]{2,1,0:T(8,128)(2,1)S(1)}) custom-call(bf16[2,4,4,48,1024]{4,3,2,1,0:T(8,128)(2,1)S(1)} %bitcast.59, bf16[128,256]{1,0:T(8,128)(2,1)S(1)} %copy.38.attn_ref), custom_call_target="tpu_custom_call" | custom-call | tf_op jit(solution)/shard_map/combine/pallas_call | solution.py:538
  121.0 0.8 convert_bitcast_fusion
  121.9 1.2 copy.39
  123.5 1.2 fusion.6
  124.7 1.0 convolution_convert_fusion.3
  (73 shorter events, 3.6 us)
Async XLA Ops:
  0.6 122.8 %copy-start = (bf16[1024,1024]{1,0:T(8,128)(2,1)S(1)}, bf16[1024,1024]{1,0:T(8,128)(2,1)}, u32[]{:S(2)}) copy-start(bf16[1024,1024]{1,0:T(8,128)(2,1)} %param.26) | copy-start | bytes 6291460
  0.6 6.9 %copy-start.8 = (bf16[128,32]{0,1:T(8,128)(2,1)S(1)}, bf16[128,32]{0,1:T(8,128)(2,1)}, u32[]{:S(2)}) copy-start(bf16[128,32]{0,1:T(8,128)(2,1)} %param.19) | copy-start | bytes 24580
  0.7 7.0 %copy-start.6 = (bf16[128,512]{1,0:T(8,128)(2,1)S(1)}, bf16[128,512]{1,0:T(8,128)(2,1)}, u32[]{:S(2)}) copy-start(bf16[128,512]{1,0:T(8,128)(2,1)} %param.18) | copy-start | bytes 393220
  0.7 43.3 %copy-start.14 = (f32[512]{0:T(512)S(1)}, f32[512]{0:T(512)}, u32[]{:S(2)}) copy-start(f32[512]{0:T(512)} %param.20) | copy-start | bytes 6148
  0.7 43.2 %copy-start.12 = (bf16[512,256]{1,0:T(8,128)(2,1)S(1)}, bf16[512,256]{1,0:T(8,128)(2,1)}, u32[]{:S(2)}) copy-start(bf16[512,256]{1,0:T(8,128)(2,1)} %param.21) | copy-start | bytes 786436
  41.1 1.7 %copy-start.2 = (bf16[4,2,4,48,1024]{4,3,2,1,0:T(8,128)(2,1)}, bf16[4,2,4,48,1024]{4,3,2,1,0:T(8,128)(2,1)S(1)}, u32[]{:S(2)}) copy-start(bf16[4,2,4,48,1024]{4,3,2,1,0:T(8,128)(2,1)S(1)} %get-tuple-element.8) | copy-start | bytes 9437188
  42.8 1.1 copy-start.3
  45.2 4.1 %copy-start.11 = (f32[96]{0:T(128)S(1)}, f32[96]{0:T(128)}, u32[]{:S(2)}) copy-start(f32[96]{0:T(128)} %param.24) | copy-start | bytes 1156
  49.3 3.7 %copy-start.7 = (bf16[128,384]{1,0:T(8,128)(2,1)S(1)}, bf16[128,384]{1,0:T(8,128)(2,1)}, u32[]{:S(2)}) copy-start(bf16[128,384]{1,0:T(8,128)(2,1)} %param.17) | copy-start | bytes 294916
  49.7 1.1 copy-start.5
  50.8 2.3 %copy-start.10 = (f32[96]{0:T(128)S(1)}, f32[96]{0:T(128)}, u32[]{:S(2)}) copy-start(f32[96]{0:T(128)} %param.23) | copy-start | bytes 1156
  54.0 1.3 %copy-start.4 = (bf16[4,2,4,32,640]{4,3,2,1,0:T(8,128)(2,1)S(1)}, bf16[4,2,4,32,640]{4,3,2,1,0:T(8,128)(2,1)}, u32[]{:S(2)}) copy-start(bf16[4,2,4,32,640]{4,3,2,1,0:T(8,128)(2,1)} %copy-done.3) | copy-start | bytes 3932164
  54.0 1.3 %copy-start.13 = (bf16[512,256]{1,0:T(8,128)(2,1)S(1)}, bf16[512,256]{1,0:T(8,128)(2,1)}, u32[]{:S(2)}) copy-start(bf16[512,256]{1,0:T(8,128)(2,1)} %param.22) | copy-start | bytes 786436
  94.7 1.9 %copy-start.1 = (bf16[8,4,48,1024]{3,2,1,0:T(8,128)(2,1)S(1)}, bf16[8,4,48,1024]{3,2,1,0:T(8,128)(2,1)}, u32[]{:S(2)}) copy-start(bf16[8,4,48,1024]{3,2,1,0:T(8,128)(2,1)} %experts.1) | copy-start | bytes 9437188
  96.6 26.6 %copy-start.9 = (f32[1024]{0:T(1024)S(1)}, f32[1024]{0:T(1024)}, u32[]{:S(2)}) copy-start(f32[1024]{0:T(1024)} %param.25) | copy-start | bytes 12292

commit v2 on v1

--- a/solution.py
+++ b/solution.py
@@ -232,14 +232,24 @@
     pl.semaphore_wait(barrier, len(peers))
 
 
-def dispatch_kernel(
+def routed_kernel(
     planes,
     out_ref,
     meta_ref,
     kv_ref,
+    gate_ref,
+    up_ref,
+    down_ref,
+    part_ref,
+    keys_ref,
     rows_ref,
     metas_ref,
-    keys_ref,
+    gates,
+    ups,
+    downs,
+    taken,
+    given,
+    ws,
     zs,
     zr,
     xs,
@@ -260,15 +270,30 @@
     ]
     for copy in local:
         copy.start()
-    for d in range(1, planes):
-        sent.append(rdma(kv_ref, keys_ref.at[tp, 0, d], zs.at[0, d], zr.at[0, d], along(d)))
-    for d in range(1, planes):
+    order = sorted(range(1, planes), key=lambda d: (min(d, planes - d), d))
+    for d in order:
         sent.append(
             rdma(meta_ref.at[d], metas_ref.at[0, d], zs.at[1, d], zr.at[1, d], along(d))
         )
         sent.append(
             rdma(out_ref.at[d], rows_ref.at[tp, 0, d], zs.at[2, d], zr.at[2, d], along(d))
         )
+    for d in order:
+        sent.append(rdma(kv_ref, keys_ref.at[tp, 0, d], zs.at[0, d], zr.at[0, d], along(d)))
+    experts = gate_ref.shape[0]
+    down_slots = downs.shape[0]
+
+    def fetch(which, source, target, expert):
+        return pltpu.make_async_copy(source, target, ws.at[which, expert])
+
+    gate_in = [fetch(0, gate_ref.at[e], gates.at[e], e) for e in range(experts)]
+    up_in = [fetch(1, up_ref.at[e], ups.at[e], e) for e in range(experts)]
+    down_in = [fetch(2, down_ref.at[e], downs.at[e % down_slots], e) for e in range(experts)]
+    for e in range(experts):
+        gate_in[e].start()
+        up_in[e].start()
+        if e < down_slots:
+            down_in[e].start()
     for copy in local:
         copy.wait()
     bufs = (keys_ref, rows_ref)
@@ -320,7 +345,7 @@
         arrived(high, xr.at[kind, 3, d], near_x)
         to_partner(kind, 3, tp ^ 3, d)
 
-    jobs = [(0, d) for d in range(planes)] + [(1, d) for d in range(planes)]
+    jobs = [(1, 0), (0, 0)] + [(1, d) for d in order] + [(0, d) for d in order]
     for step in range(len(jobs) + 4):
         if step < len(jobs):
             first(*jobs[step])
@@ -333,23 +358,91 @@
             for which, flip in enumerate((0, 1, 2, 3)):
                 arrived(bufs[kind].at[tp ^ flip, 1, d], pr.at[kind, which, d], partner)
         arrived(metas_ref.at[1, d], pr.at[2, 0, d], partner)
+
+    f32, bf = jnp.float32, jnp.bfloat16
+    core = lax.axis_index("ep") % 2
+    parts, width = part_ref.shape[1], part_ref.shape[3]
+    cap = out_ref.shape[1]
+    blocks = 2 * planes
+    row_total, slots = blocks * cap, blocks * CAP
+    info = metas_ref[...].reshape(row_total, PAD)
+    codes = info.astype(f32)
+    block_of = lax.broadcasted_iota(jnp.int32, (blocks, cap, 1), 0).reshape(row_total, 1)
+    slot_ids = lax.broadcasted_iota(jnp.int32, (row_total, experts * slots), 1)
+    match = []
+    for pick in range(2):
+        code = codes[:, pick : pick + 1].astype(jnp.int32) - 1 - core * (experts * CAP)
+        inside = (codes[:, pick : pick + 1] > 0.5) & (code >= 0) & (code < experts * CAP)
+        expert = jnp.zeros_like(code)
+        for e in range(1, experts):
+            expert += (code >= e * CAP).astype(jnp.int32)
+        where = expert * (slots - CAP) + block_of * CAP + code
+        match.append((slot_ids == jnp.where(inside, where, -1)).astype(f32).astype(bf))
+    place = match[0] + match[1]
+    turned = (((0,), (0,)), ((), ()))
+    weights = jnp.zeros((experts * slots, 1), f32)
+    for pick in range(2):
+        found = lax.dot_general(match[pick], info, turned, preferred_element_type=f32)
+        weights += found[:, 2 + pick : 3 + pick] + found[:, 4 + pick : 5 + pick]
+    for q in range(parts):
+        rows = rows_ref[q].reshape(row_total, width)
+        taken[:, q * width : (q + 1) * width] = lax.dot_general(
+            place, rows, turned, preferred_element_type=f32
+        ).astype(bf)
+    for e in range(experts):
+        first_slot = e * slots
+        picked = taken[first_slot : first_slot + slots, :]
+        gate_in[e].wait()
+        gate = jnp.dot(picked, gates[e], preferred_element_type=f32)
+        up_in[e].wait()
+        upper = jnp.dot(picked, ups[e], preferred_element_type=f32)
+        hidden = (
+            gate / (1.0 + jnp.exp(-gate)) * upper * weights[first_slot : first_slot + slots]
+        ).astype(bf)
+        down_in[e].wait()
+        for q in range(parts):
+            given[first_slot : first_slot + slots, q * width : (q + 1) * width] = jnp.dot(
+                hidden,
+                downs[e % down_slots, :, q * width : (q + 1) * width],
+                preferred_element_type=f32,
+            ).astype(bf)
+        if e + down_slots < experts:
+            down_in[e + down_slots].start()
+    for q in range(parts):
+        back = jnp.dot(
+            place, given[:, q * width : (q + 1) * width], preferred_element_type=f32
+        )
+        part_ref[:, q] = back.astype(bf).reshape(blocks, cap, width)
     for copy in sent:
         copy.wait_send()
 
 
-def dispatch(outgoing, metas, kv_part, tp_count):
+def routed(outgoing, metas, kv_part, w_gate, w_up, w_down, tp_count):
     planes, cap, width = outgoing.shape
+    experts, model, hidden = w_gate.shape
+    blocks = 2 * planes
+    slot_total = experts * blocks * CAP
     dma = pltpu.SemaphoreType.DMA
+    bf = jnp.bfloat16
+    vmem = pl.BlockSpec(memory_space=pltpu.VMEM)
+    hbm = pl.BlockSpec(memory_space=pl.ANY)
     return pl.pallas_call(
-        functools.partial(dispatch_kernel, planes),
+        functools.partial(routed_kernel, planes),
         out_shape=(
-            jax.ShapeDtypeStruct((tp_count, 2, planes, cap, width), jnp.bfloat16),
-            jax.ShapeDtypeStruct((2, planes, cap, PAD), jnp.bfloat16),
-            jax.ShapeDtypeStruct((tp_count, 2, planes) + kv_part.shape, jnp.bfloat16),
+            jax.ShapeDtypeStruct((blocks, tp_count, cap, width), bf),
+            jax.ShapeDtypeStruct((tp_count, 2, planes) + kv_part.shape, bf),
         ),
-        in_specs=[pl.BlockSpec(memory_space=pltpu.VMEM)] * 3,
-        out_specs=(pl.BlockSpec(memory_space=pltpu.VMEM),) * 3,
+        in_specs=[vmem] * 3 + [hbm] * 3,
+        out_specs=(vmem,) * 2,
         scratch_shapes=[
+            pltpu.VMEM((tp_count, 2, planes, cap, width), bf),
+            pltpu.VMEM((2, planes, cap, PAD), bf),
+            pltpu.VMEM((experts, model, hidden), bf),
+            pltpu.VMEM((experts, model, hidden), bf),
+            pltpu.VMEM((2, hidden, model), bf),
+            pltpu.VMEM((slot_total, model), bf),
+            pltpu.VMEM((slot_total, model), bf),
+            dma((3, experts)),
             dma((3, planes)),
             dma((3, planes)),
             dma((2, 4, planes)),
@@ -359,88 +452,10 @@
             dma((3,)),
         ],
         compiler_params=pltpu.CompilerParams(
-            collective_id=0, has_side_effects=True, vmem_limit_bytes=40 * 2**20
+            collective_id=0, has_side_effects=True, vmem_limit_bytes=67043328
         ),
-        name="dispatch",
-    )(outgoing, metas, kv_part)
-
-
-def expert_kernel(
-    pick_ref, place_ref, weight_ref, rows_ref, gate_ref, up_ref, down_ref, out_ref, g_acc, u_acc, total
-):
-    expert = pl.program_id(0)
-    quarter = pl.program_id(1)
-    experts = pl.num_programs(0)
-    quarters = pl.num_programs(1)
-
-    picked = jnp.dot(
-        pick_ref[...], rows_ref[quarter], preferred_element_type=jnp.float32
-    ).astype(jnp.bfloat16)
-    gate = jnp.dot(picked, gate_ref[...], preferred_element_type=jnp.float32)
-    upper = jnp.dot(picked, up_ref[...], preferred_element_type=jnp.float32)
-
-    @pl.when(quarter == 0)
-    def _():
-        g_acc[...] = gate
-        u_acc[...] = upper
-
-    @pl.when(quarter > 0)
-    def _():
-        g_acc[...] += gate
-        u_acc[...] += upper
-
-    @pl.when(quarter == quarters - 1)
-    def _():
-        g = g_acc[...]
-        hidden = (g / (1.0 + jnp.exp(-g)) * u_acc[...] * weight_ref[...]).astype(jnp.bfloat16)
-        blocks, parts, cap, width = out_ref.shape
-        for q in range(parts):
-            y = jnp.dot(
-                hidden, down_ref[:, q * width : (q + 1) * width], preferred_element_type=jnp.float32
-            ).astype(jnp.bfloat16)
-            back = jnp.dot(place_ref[...], y, preferred_element_type=jnp.float32)
-
-            @pl.when(expert == 0)
-            def _():
-                total[q] = back
-
-            @pl.when(expert > 0)
-            def _():
-                total[q] += back
-
-            @pl.when(expert == experts - 1)
-            def _():
-                out_ref[:, q] = total[q].reshape(blocks, cap, width).astype(jnp.bfloat16)
-
-
-def run_experts(pick, place, weights, rows, w_gate, w_up, w_down, blocks, cap):
-    experts, slots, row_count = pick.shape
-    parts, _, width = rows.shape
-    hidden = w_gate.shape[2]
-    return pl.pallas_call(
-        expert_kernel,
-        grid=(experts, parts),
-        out_shape=jax.ShapeDtypeStruct((blocks, parts, cap, width), jnp.bfloat16),
-        in_specs=[
-            pl.BlockSpec((None, slots, row_count), lambda e, q: (e, 0, 0)),
-            pl.BlockSpec((None, row_count, slots), lambda e, q: (e, 0, 0)),
-            pl.BlockSpec((None, slots, 1), lambda e, q: (e, 0, 0)),
-            pl.BlockSpec((parts, row_count, width), lambda e, q: (0, 0, 0)),
-            pl.BlockSpec((None, width, hidden), lambda e, q: (e, q, 0)),
-            pl.BlockSpec((None, width, hidden), lambda e, q: (e, q, 0)),
-            pl.BlockSpec((None, hidden, parts * width), lambda e, q: (e, 0, 0)),
-        ],
-        out_specs=pl.BlockSpec((blocks, parts, cap, width), lambda e, q: (0, 0, 0, 0)),
-        scratch_shapes=[
-            pltpu.VMEM((slots, hidden), jnp.float32),
-            pltpu.VMEM((slots, hidden), jnp.float32),
-            pltpu.VMEM((parts, row_count, width), jnp.float32),
-        ],
-        compiler_params=pltpu.CompilerParams(
-            dimension_semantics=("arbitrary", "arbitrary"), vmem_limit_bytes=56 * 2**20
-        ),
-        name="experts",
-    )(pick, place, weights, rows, w_gate, w_up, w_down)
+        name="routed",
+    )(outgoing, metas, kv_part, w_gate, w_up, w_down)
 
 
 def combine_kernel(
@@ -594,9 +609,7 @@
     plane, core = ep // 2, ep % 2
     tokens, model = moe_input.shape
     width = model // tp_count
-    local_experts = w_gate.shape[0]
     cap = group_cap()
-    blocks = 2 * planes
 
     group = expert_ids[:, 0] // GROUP
     offset = lax.rem(group - plane + planes, planes)
@@ -635,43 +648,16 @@
         jnp.concatenate([kv_latent, rope_key], axis=1), ((0, 0), (0, PAD - ROPE))
     )
     kv_part = lax.dynamic_slice_in_dim(kv_all, tp * kv_rows, kv_rows, 0)
-    rows, metas, keys = dispatch(
-        outgoing.reshape(planes, cap, width), metas_out.reshape(planes, cap, PAD), kv_part, tp_count
-    )
-
-    row_total = blocks * cap
-    slots = blocks * CAP
-    info = metas.reshape(row_total, PAD)[:, :6].astype(f32)
-    block_of = jnp.arange(row_total, dtype=jnp.int32) // cap
-    positions = []
-    for k in range(2):
-        code = info[:, k].astype(jnp.int32) - 1 - core * (local_experts * CAP)
-        inside = (info[:, k] > 0.5) & (code >= 0) & (code < local_experts * CAP)
-        where = (code // CAP) * slots + block_of * CAP + code % CAP
-        positions.append(jnp.where(inside, where, -1))
-    slot_ids = jnp.arange(local_experts * slots, dtype=jnp.int32).reshape(local_experts, slots)
-    match = [slot_ids[:, :, None] == positions[k][None, None, :] for k in range(2)]
-    pick = (match[0] | match[1]).astype(bf)
-    flip = [slot_ids[:, None, :] == positions[k][None, :, None] for k in range(2)]
-    place = (flip[0] | flip[1]).astype(bf)
-    weight_of = [info[:, 2 + k] + info[:, 4 + k] for k in range(2)]
-    weights = jnp.sum(
-        jnp.where(match[0], weight_of[0][None, None, :], 0.0)
-        + jnp.where(match[1], weight_of[1][None, None, :], 0.0),
-        axis=2,
-        keepdims=True,
-    )
-    partial = run_experts(
-        pick,
-        place,
-        weights,
-        rows.reshape(tp_count, row_total, width),
+    partial, keys = routed(
+        outgoing.reshape(planes, cap, width),
+        metas_out.reshape(planes, cap, PAD),
+        kv_part,
         w_gate,
         w_up,
         w_down,
-        blocks,
-        cap,
-    ).reshape(2, planes, tp_count, cap, width)
+        tp_count,
+    )
+    partial = partial.reshape(2, planes, tp_count, cap, width)
 
     tok_rows = queries.shape[0]
     head_count = key_up.shape[1] // NOPE

time: 126 us -> 100 us (0.79)
  Pallas kernels: 92.5 us -> 74.4 us
  local copies, waits for them, and re-layouts: 13.5 us -> 5.28 us
  matrix products: 7.09 us -> 9.99 us
  other arithmetic: 11.5 us -> 9.19 us
    pallas_call x2 -> x1, Pallas kernels: 68.1 us -> 49.8 us  [routed(): pl.pallas_call(functools.partial(routed_kernel, planes), out_shape=(jax.S...]
    unnamed x33 -> x34, local copies, waits for them, and re-layouts: 7.24 us -> 3.72 us
    dot_general x1, matrix products: 0.67 us -> 2.77 us  [make_keys(): jnp.dot(latent_n, value_up, preferred_element_type=jnp.float32)]
    convert_element_type x3 -> x0, other arithmetic: 1.82 us -> none  [the longest x1 0.94 us: grouped_shards(): place = (flip[0] | flip[1]).astype(bf)]
    reduce_sum x1, other arithmetic: 0.27 us -> 1.6 us  [make_keys(): jnp.mean(latent_f * latent_f, axis=-1, keepdims=True) + EPS]
where the time goes in v2:
time: 100 us; the launch traced here: 99.9 us
  Pallas kernels  74.4 us (74%)
  matrix products  9.99 us (10%)
  other arithmetic  9.19 us (9%)
  local copies, waits for them, and re-layouts  5.28 us (5%)
  between operations  1.01 us (1%)
    pallas_call x1, Pallas kernels, routed(): pl.pallas_call(functools.partial(routed_kernel, planes), out_shape=(jax.S...  49.8 us
    pallas_call x1, Pallas kernels, combine(): pl.pallas_call(functools.partial(combine_kernel, planes), out_shape=(jax....  24.6 us
    unnamed x34, local copies, waits for them, and re-layouts  3.72 us
    dot_general x1, matrix products, make_keys(): jnp.dot(latent_n, value_up, preferred_element_type=jnp.float32)  2.77 us
    dot_general x1, matrix products, grouped_shards(): outgoing = jnp.dot(select, normed, preferred_element_type=f32).astype(bf)  2.05 us

profile of v2, /device:TPU:0, one launch (start us, length us, event | category | flops | bytes accessed | tf_op | source)
XLA Modules:
  0.0 99.9 jit_solution(14108931584072933940)
XLA Ops:
  0.7 0.7 dynamic_slice.10
  1.4 1.5 %multiply_reduce_fusion = f32[128]{0:T(128)S(1)} fusion(bf16[128,4096]{1,0:T(8,128)(2,1)} %param.27), kind=kLoop, calls=%fused_computation.7 | loop fusion | flops 1572736 | bytes 1049088 | tf_op jit(solution)/shard_map/reduce_sum | solution.py:639
  2.9 0.7 and_select_fusion
  3.6 0.7 add_bitcast_fusion.1
  4.3 0.1 fusion.37
  4.5 0.7 fusion.65
  5.2 2.1 %convolution_convert_fusion.2 = bf16[192,1024]{1,0:T(8,128)(2,1)} fusion(f32[1024]{0:T(1024)S(1)} %dynamic_slice.10, f32[128]{0:T(128)S(1)} %add_rsqrt_fusion.4, bf16[128,4096]{1,0:T(8,128)(2,1)} %param.27, s32[]{:T(128)S(6)} %select_n.57, s32[128]{0:T(128)S(1)} %fusion.65), kind=kOutput, calls=%fused_computation.16 | convolution fusion | flops 51077120 | bytes 660484 | tf_op jit(solution)/shard_map/dot_general | solution.py:643
  7.3 0.7 reduce-precision_convert_fusion
  8.0 0.8 convolution_convert_fusion.4
  8.9 0.6 fusion.41.kv_ref
  9.5 49.8 %routed.1 = (bf16[8,4,48,1024]{3,2,1,0:T(8,128)(2,1)}, bf16[4,2,4,32,640]{4,3,2,1,0:T(8,128)(2,1)}) custom-call(bf16[4,48,1024]{2,1,0:T(8,128)(2,1)} %bitcast.61, bf16[4,48,128]{2,1,0:T(8,128)(2,1)} %bitcast.67, bf16[32,640]{1,0:T(8,128)(2,1)} %fusion.41.kv_ref, bf16[4,4096,512]{2,1,0:T(8,128)(2,1)} %gate_ref.1, bf16[4,4096,512]{2,1,0:T(8,128)(2,1)} %up_ref.1, ...), custom_call_target="tpu_custom_call" | custom-call | tf_op jit(solution)/shard_map/routed/pallas_call | solution.py:429
  59.4 1.6 %fusion = f32[1024]{0:T(1024)S(1)} fusion(bf16[1024,640]{1,0:T(8,128)(2,1)} %bitcast.62), kind=kLoop, calls=%fused_computation.2 | loop fusion | flops 1571840 | bytes 1052672 | tf_op jit(solution)/shard_map/reduce_sum | solution.py:59
  61.0 2.8 %convolution_convert_fusion = bf16[1024,256]{0,1:T(8,128)(2,1)} fusion(bf16[512,256]{1,0:T(8,128)(2,1)} %param.22, f32[512]{0:T(512)} %param.20, f32[1024]{0:T(1024)S(1)} %add_rsqrt_fusion.1, bf16[1024,640]{1,0:T(8,128)(2,1)} %bitcast.63), kind=kOutput, calls=%fused_computation.14 | convolution fusion | flops 270794752 | bytes 1841152 | tf_op jit(solution)/shard_map/dot_general | solution.py:64
  64.1 0.1 broadcast_compare_fusion
  64.5 0.7 convolution_convert_fusion.1
  65.2 0.2 copy.32
  65.4 0.2 multiply_reduce_fusion.1
  65.6 0.2 copy-done.12
  65.9 0.4 multiply_multiply_fusion
  66.3 0.3 multiply_cosine_fusion
  67.2 0.7 fusion.3
  67.9 0.6 fusion.4
  68.5 0.4 copy-done.15
  68.9 0.7 fusion.8
  69.8 1.0 %copy-done = bf16[8,4,48,1024]{3,2,1,0:T(8,128)(2,1)S(1)} copy-done((bf16[8,4,48,1024]{3,2,1,0:T(8,128)(2,1)S(1)}, bf16[8,4,48,1024]{3,2,1,0:T(8,128)(2,1)}, u32[]{:S(2)}) %copy-start) | copy-done | bytes 3145752
  70.8 24.6 %combine.1 = (bf16[4,48,1024]{2,1,0:T(8,128)(2,1)S(1)}, bf16[4,128,256]{2,1,0:T(8,128)(2,1)S(1)}) custom-call(bf16[2,4,4,48,1024]{4,3,2,1,0:T(8,128)(2,1)S(1)} %bitcast.55, bf16[128,256]{1,0:T(8,128)(2,1)S(1)} %copy.34.attn_ref), custom_call_target="tpu_custom_call" | custom-call | tf_op jit(solution)/shard_map/combine/pallas_call | solution.py:553
  95.4 0.7 copy-done.1
  96.2 0.2 copy.35
  96.4 0.2 fusion.20
  96.8 1.0 copy-done.3
  97.8 1.2 %fusion.6 = bf16[128,1024]{1,0:T(8,128)(2,1)} fusion(bf16[128,1024]{0,1:T(8,128)(2,1)S(1)} %fusion.20, bf16[1024,1024]{1,0:T(8,128)(2,1)S(1)} %copy-done.3, f32[128]{0:T(128)S(1)} %add_rsqrt_fusion.3), kind=kOutput, calls=%fused_computation.19 | convolution fusion | flops 268697600 | bytes 2621952 | tf_op jit(solution)/shard_map/dot_general | solution.py:701
  98.9 1.0 convolution_convert_fusion.3
  (63 shorter events, 1.6 us)
Async XLA Ops:
  0.6 8.3 %copy-start.5 = (bf16[128,512]{1,0:T(8,128)(2,1)S(1)}, bf16[128,512]{1,0:T(8,128)(2,1)}, u32[]{:S(2)}) copy-start(bf16[128,512]{1,0:T(8,128)(2,1)} %param.18) | copy-start | bytes 393220
  0.6 8.1 %copy-start.7 = (bf16[128,32]{0,1:T(8,128)(2,1)S(1)}, bf16[128,32]{0,1:T(8,128)(2,1)}, u32[]{:S(2)}) copy-start(bf16[128,32]{0,1:T(8,128)(2,1)} %param.19) | copy-start | bytes 24580
  5.2 3.5 %copy-start.8 = (s32[128]{0:T(128)}, s32[128]{0:T(128)S(1)}, u32[]{:S(2)}) copy-start(s32[128]{0:T(128)S(1)} %fusion.65) | copy-start | bytes 1540
  59.4 4.9 %copy-start.4 = (bf16[4,2,4,32,640]{4,3,2,1,0:T(8,128)(2,1)S(1)}, bf16[4,2,4,32,640]{4,3,2,1,0:T(8,128)(2,1)}, u32[]{:S(2)}) copy-start(bf16[4,2,4,32,640]{4,3,2,1,0:T(8,128)(2,1)} %get-tuple-element.7) | copy-start | bytes 3932164
  61.0 3.5 %copy-start.13 = (bf16[512,256]{1,0:T(8,128)(2,1)S(1)}, bf16[512,256]{1,0:T(8,128)(2,1)}, u32[]{:S(2)}) copy-start(bf16[512,256]{1,0:T(8,128)(2,1)} %param.21) | copy-start | bytes 786436
  61.0 3.5 %copy-start.14 = (f32[512]{0:T(512)S(1)}, f32[512]{0:T(512)}, u32[]{:S(2)}) copy-start(f32[512]{0:T(512)} %param.20) | copy-start | bytes 6148
  65.2 0.7 copy-start.12
  65.9 0.9 copy-start.6
  66.3 0.7 copy-start.11
  67.9 1.0 %copy-start.15 = (bf16[1024,256]{0,1:T(8,128)(2,1)S(1)}, bf16[1024,256]{0,1:T(8,128)(2,1)}, u32[]{:S(2)}) copy-start(bf16[1024,256]{0,1:T(8,128)(2,1)} %convolution_convert_fusion) | copy-start | bytes 1572868
  68.9 1.9 %copy-start = (bf16[8,4,48,1024]{3,2,1,0:T(8,128)(2,1)S(1)}, bf16[8,4,48,1024]{3,2,1,0:T(8,128)(2,1)}, u32[]{:S(2)}) copy-start(bf16[8,4,48,1024]{3,2,1,0:T(8,128)(2,1)} %get-tuple-element.6) | copy-start | bytes 9437188
  70.8 25.6 %copy-start.10 = (f32[1024]{0:T(1024)S(1)}, f32[1024]{0:T(1024)}, u32[]{:S(2)}) copy-start(f32[1024]{0:T(1024)} %param.25) | copy-start | bytes 12292
  95.4 0.7 copy-start.1
  96.2 1.6 %copy-start.3 = (bf16[1024,1024]{1,0:T(8,128)(2,1)S(1)}, bf16[1024,1024]{1,0:T(8,128)(2,1)}, u32[]{:S(2)}) copy-start(bf16[1024,1024]{1,0:T(8,128)(2,1)} %param.26) | copy-start | bytes 6291460
  96.4 2.5 %copy-start.2 = (bf16[4,48,1024]{2,1,0:T(8,128)(2,1)S(1)}, bf16[4,48,1024]{2,1,0:T(8,128)(2,1)}, u32[]{:S(2)}) copy-start(bf16[4,48,1024]{2,1,0:T(8,128)(2,1)} %copy-done.1) | copy-start | bytes 1179652
  96.4 2.5 %copy-start.9 = (s32[128]{0:T(128)S(1)}, s32[128]{0:T(128)}, u32[]{:S(2)}) copy-start(s32[128]{0:T(128)} %copy-done.8) | copy-start | bytes 1540
